TPU v7x, 32 devices: a whole 2x2x4 slice. The times are simulated.
32 devices in a mesh: gr: 2 (over x), fs: 4 (over z), tp: 4 (over y, core).
Axes of the slice: x: 2, y: 2, z: 4, core: 2. Of those that a mesh axis runs over, the one named last changes fastest.
Arguments:
- tokens: bfloat16 [4096, 2048], P(('gr', 'fs', 'tp')), may hold values from -6 to 6
- norm_gain: float32 [2048], P('fs'), may hold values from 0.1 to 1.9
- gate_master: float32 [16, 2048, 256], P(None, 'fs', ('gr', 'tp')), may hold values from -0.125 to 0.125
- up_master: float32 [16, 2048, 256], P(None, 'fs', ('gr', 'tp')), may hold values from -0.125 to 0.125
- down_master: float32 [16, 256, 2048], P(None, 'fs', ('gr', 'tp')), may hold values from -0.375 to 0.375
- route_group: int32 [4096], P(('gr', 'fs', 'tp')), may hold values from 0 to 3
- route_expert: int32 [4096, 2], P(('gr', 'fs', 'tp')), may hold values from 0 to 3, all different within a row
- route_weight: float32 [4096, 2], P(('gr', 'fs', 'tp')), may hold values from 0.1 to 1
Outputs:
- gate_new: bfloat16 [16, 2048, 256], P(('fs', 'tp'))
- up_new: bfloat16 [16, 2048, 256], P(('fs', 'tp'))
- down_new: bfloat16 [16, 256, 2048], P(('fs', 'tp'))
- mixed: bfloat16 [4096, 2048], P(('gr', 'fs', 'tp'))
Inputs may be any that keep to these rules, and one draw needn't show every extreme that they name: `route_expert`: the 2 entries of a row are different.
All inputs are finite; a program needn't handle non-finite values.
Results may differ from a plain program's by a relative error of at most 0.0086.
Values may be sent and summed in bfloat16 or wider, within the bound.
A program may use at most 64 MiB of HBM per device.

v0:
```python
import jax
import jax.numpy as jnp
from jax import lax
from jax.sharding import PartitionSpec as P

E_GROUPS = 4
TOP = 2


def body(
    tokens, norm_gain, gate_master, up_master, down_master, route_group, route_expert, route_weight
):
    n_fs = lax.axis_size("fs")
    n_tp = lax.axis_size("tp")
    n_gr = lax.axis_size("gr")
    experts = n_fs * n_tp
    per_group = experts // E_GROUPS
    gate_cast = (gate_master * norm_gain[None, :, None]).astype(jnp.bfloat16)
    up_cast = (up_master * norm_gain[None, :, None]).astype(jnp.bfloat16)
    down_cast = down_master.astype(jnp.bfloat16)

    def to_grid(tile):
        return tile.reshape((n_fs, n_tp, 1, tile.shape[1], tile.shape[2]))

    grids = (
        to_grid(jnp.swapaxes(gate_cast, 1, 2)),
        to_grid(jnp.swapaxes(up_cast, 1, 2)),
        to_grid(down_cast),
    )
    grids = (
        lax.all_to_all(
            lax.all_to_all(grids[0], "fs", split_axis=0, concat_axis=4, tiled=True),
            "tp",
            split_axis=1,
            concat_axis=3,
            tiled=True,
        ),
        lax.all_to_all(
            lax.all_to_all(grids[1], "fs", split_axis=0, concat_axis=4, tiled=True),
            "tp",
            split_axis=1,
            concat_axis=3,
            tiled=True,
        ),
        lax.all_to_all(
            lax.all_to_all(grids[2], "fs", split_axis=0, concat_axis=4, tiled=True),
            "tp",
            split_axis=1,
            concat_axis=3,
            tiled=True,
        ),
    )
    grids = (
        lax.all_gather(grids[0], "gr", axis=2, tiled=True),
        lax.all_gather(grids[1], "gr", axis=2, tiled=True),
        lax.all_gather(grids[2], "gr", axis=2, tiled=True),
    )

    def rows_to_matrix(grid):
        hidden_units = grid.shape[2] * grid.shape[3]
        return jnp.swapaxes(grid.reshape(hidden_units, grid.shape[4]), 0, 1)[None]

    gate_new = rows_to_matrix(grids[0])
    up_new = rows_to_matrix(grids[1])
    grid = grids[2]
    f_local = grid.shape[3] // n_tp
    d_local = grid.shape[4] // n_fs
    parts = grid.reshape(n_gr, n_tp, f_local, n_fs, d_local)
    parts = jnp.transpose(parts, (3, 2, 0, 1, 4))
    down_new = parts.reshape(1, n_fs * f_local, n_gr * n_tp * d_local)
    width = tokens.shape[1]
    count = tokens.shape[0]
    floats = tokens.astype(jnp.float32)
    normed = (floats * lax.rsqrt(jnp.mean(floats * floats, axis=-1, keepdims=True) + 1e-06)).astype(
        jnp.bfloat16
    )
    capacity = 3 * count * TOP // (2 * experts)
    flat_ids = (route_group[:, None] * per_group + route_expert).reshape(-1)
    columns = lax.broadcasted_iota(jnp.int32, (flat_ids.shape[0], experts), 1)
    onehot = (flat_ids[:, None] == columns).astype(jnp.int32)
    rank = jnp.sum((jnp.cumsum(onehot, axis=0) - 1) * onehot, axis=1)
    dump = experts * capacity
    slot = jnp.where(rank < capacity, flat_ids * capacity + rank, dump)
    rows = jnp.repeat(normed, TOP, axis=0)
    outgoing = (
        jnp.zeros((dump + 1, width), jnp.bfloat16)
        .at[slot]
        .set(rows)[:-1]
        .reshape(experts, capacity, width)
    )
    block = lax.all_to_all(outgoing, ("fs", "tp"), split_axis=0, concat_axis=0, tiled=True)
    flat_rows = block.reshape(-1, width)
    gate = jnp.dot(flat_rows, gate_new[0], preferred_element_type=jnp.float32)
    upper = jnp.dot(flat_rows, up_new[0], preferred_element_type=jnp.float32)
    hidden = (jax.nn.silu(gate) * upper).astype(jnp.bfloat16)
    result = jnp.dot(hidden, down_new[0], preferred_element_type=jnp.float32).astype(jnp.bfloat16)
    outcome = result.reshape(block.shape)
    returned = lax.all_to_all(outcome, ("fs", "tp"), split_axis=0, concat_axis=0, tiled=True)
    table = jnp.concatenate(
        [returned.reshape(-1, width), jnp.zeros((1, width), jnp.bfloat16)], axis=0
    )
    picked = table[slot].reshape(count, TOP, width).astype(jnp.float32)
    mixed = jnp.sum(picked * route_weight[:, :, None], axis=1).astype(jnp.bfloat16)
    return (gate_new, up_new, down_new, mixed)


def solution(mesh):
    placed = (
        P(("gr", "fs", "tp"), None),
        P("fs"),
        P(None, "fs", ("gr", "tp")),
        P(None, "fs", ("gr", "tp")),
        P(None, "fs", ("gr", "tp")),
        P(("gr", "fs", "tp")),
        P(("gr", "fs", "tp"), None),
        P(("gr", "fs", "tp"), None),
    )
    return jax.shard_map(
        body,
        mesh=mesh,
        in_specs=placed,
        out_specs=(
            P(("fs", "tp"), None, None),
            P(("fs", "tp"), None, None),
            P(("fs", "tp"), None, None),
            P(("gr", "fs", "tp"), None),
        ),
        check_vma=False,
    )
```

profile of v0, /device:TPU:13, one launch (start us, length us, event | category | flops | bytes accessed | tf_op | source)
XLA Modules:
  0.0 240.0 jit_solution(1093380789958716760)
XLA Ops:
  7.2 2.6 %multiply_convert_fusion = (bf16[16,512,32]{1,2,0:T(8,128)(2,1)}, bf16[16,512,32]{1,2,0:T(8,128)(2,1)S(1)}) fusion(f32[16,512,32]{1,2,0:T(8,128)} %param.11, f32[512]{0:T(512)} %param.9, f32[16,512,32]{1,2,0:T(8,128)} %param.10), kind=kLoop, calls=%fused_computation.10 | loop fusion | flops 1048576 | bytes 3147776 | tf_op jit(solution)/shard_map/convert_element_type | solution.py:19
  9.8 16.6 %all_to_all.100 = bf16[4,4,1,32,512]{4,3,1,2,0:T(8,128)(2,1)S(1)} all-to-all(bf16[4,4,1,32,512]{4,3,1,2,0:T(8,128)(2,1)S(1)} %bitcast.88), channel_id=1, replica_groups=mesh['gr'=2,'fs'=4,'tp'=4] {'fs'}, dimensions={0} | all-to-all | bytes 1048576 | tf_op jit(solution)/shard_map/all_to_all | solution.py:32
  26.4 5.3 %all-to-all-start.2 = ((bf16[4,4,1,32,512]{4,3,1,2,0:T(8,128)(2,1)}), bf16[4,4,1,32,512]{4,3,1,2,0:T(8,128)(2,1)S(1)}, u32[]{:S(2)}, u32[]{:S(2)}) async-start(bf16[4,4,1,32,512]{4,3,1,2,0:T(8,128)(2,1)} %bitcast.11), calls=%async_computation.2 | async-start | bytes 1048576 | tf_op jit(solution)/shard_map/all_to_all | solution.py:39
  31.7 0.0 copy-done.4
  31.7 0.9 convert_element_type.37
  32.6 9.8 %all-to-all-done.2 = bf16[4,4,1,32,512]{4,3,1,2,0:T(8,128)(2,1)S(1)} async-done(((bf16[4,4,1,32,512]{4,3,1,2,0:T(8,128)(2,1)}), bf16[4,4,1,32,512]{4,3,1,2,0:T(8,128)(2,1)S(1)}, u32[]{:S(2)}, u32[]{:S(2)}) %all-to-all-start.2) | async-done | bytes 524320 | tf_op jit(solution)/shard_map/all_to_all | solution.py:39
  42.4 7.0 %all-to-all-start.4 = ((bf16[4,4,1,64,256]{4,3,1,2,0:T(8,128)(2,1)}), bf16[4,4,1,64,256]{4,3,1,2,0:T(8,128)(2,1)S(1)}, u32[]{:S(2)}, u32[]{:S(2)}) async-start(bf16[4,4,1,64,256]{4,3,1,2,0:T(8,128)(2,1)} %bitcast.20), calls=%async_computation.4 | async-start | bytes 1048576 | tf_op jit(solution)/shard_map/all_to_all | solution.py:46
  49.4 0.0 copy-done.7
  49.4 0.0 copy-done.6
  49.4 0.1 copy.47
  49.5 0.1 eq.21
  49.6 0.9 copy.53
  50.5 9.5 %all-to-all-done.4 = bf16[4,4,1,64,256]{4,3,1,2,0:T(8,128)(2,1)S(1)} async-done(((bf16[4,4,1,64,256]{4,3,1,2,0:T(8,128)(2,1)}), bf16[4,4,1,64,256]{4,3,1,2,0:T(8,128)(2,1)S(1)}, u32[]{:S(2)}, u32[]{:S(2)}) %all-to-all-start.4) | async-done | bytes 524320 | tf_op jit(solution)/shard_map/all_to_all | solution.py:46
  60.0 5.4 %all-to-all-start.1 = ((bf16[1,4,1,32,2048]{4,3,2,0,1:T(8,128)(2,1)}), bf16[1,4,1,32,2048]{4,3,2,0,1:T(8,128)(2,1)S(1)}, u32[]{:S(2)}, u32[]{:S(2)}) async-start(bf16[1,4,1,32,2048]{4,3,2,0,1:T(8,128)(2,1)} %bitcast.4), calls=%async_computation.1 | async-start | bytes 1048576 | tf_op jit(solution)/shard_map/all_to_all | solution.py:31
  65.4 0.6 reduce-window.6
  66.0 0.0 copy-done.1
  66.0 0.2 fusion.1
  66.2 0.9 copy.54
  67.0 5.3 %all-to-all-done.1 = bf16[1,4,1,32,2048]{4,3,2,0,1:T(8,128)(2,1)S(1)} async-done(((bf16[1,4,1,32,2048]{4,3,2,0,1:T(8,128)(2,1)}), bf16[1,4,1,32,2048]{4,3,2,0,1:T(8,128)(2,1)S(1)}, u32[]{:S(2)}, u32[]{:S(2)}) %all-to-all-start.1) | async-done | bytes 524320 | tf_op jit(solution)/shard_map/all_to_all | solution.py:31
  72.4 5.3 %all-to-all-start.3 = ((bf16[1,4,1,32,2048]{4,3,2,0,1:T(8,128)(2,1)}), bf16[1,4,1,32,2048]{4,3,2,0,1:T(8,128)(2,1)S(1)}, u32[]{:S(2)}, u32[]{:S(2)}) async-start(bf16[1,4,1,32,2048]{4,3,2,0,1:T(8,128)(2,1)} %bitcast.87), calls=%async_computation.3 | async-start | bytes 1048576 | tf_op jit(solution)/shard_map/all_to_all | solution.py:38
  77.6 0.2 fusion.2
  77.8 0.9 copy.55
  78.7 6.0 %all-to-all-done.3 = bf16[1,4,1,32,2048]{4,3,2,0,1:T(8,128)(2,1)S(1)} async-done(((bf16[1,4,1,32,2048]{4,3,2,0,1:T(8,128)(2,1)}), bf16[1,4,1,32,2048]{4,3,2,0,1:T(8,128)(2,1)S(1)}, u32[]{:S(2)}, u32[]{:S(2)}) %all-to-all-start.3) | async-done | bytes 524320 | tf_op jit(solution)/shard_map/all_to_all | solution.py:38
  84.6 0.0 copy-done.2
  84.6 5.9 %all-to-all-start.5 = ((bf16[1,4,1,64,1024]{4,3,2,0,1:T(8,128)(2,1)}), bf16[1,4,1,64,1024]{4,3,2,0,1:T(8,128)(2,1)}, u32[]{:S(2)}, u32[]{:S(2)}) async-start(bf16[1,4,1,64,1024]{4,3,2,0,1:T(8,128)(2,1)} %bitcast.23), calls=%async_computation.5 | async-start | bytes 1048576 | tf_op jit(solution)/shard_map/all_to_all | solution.py:45
  90.6 0.2 slice_reduce_fusion
  90.8 0.1 eq.18
  90.9 0.1 copy.50
  91.0 0.1 mul.70
  91.2 0.6 broadcast_in_dim.28
  91.8 0.4 reshape.146
  92.3 0.0 copy-done.3
  92.3 0.1 fusion.12
  92.4 2.6 %scatter_custom_fusion = bf16[385,2048]{1,0:T(8,128)(2,1)S(1)} fusion(s32[256]{0:T(256)S(1)} %bitcast.94, bf16[256,2048]{1,0:T(8,128)(2,1)S(1)} %reshape.146, bf16[]{:T(256)} %constant.11.clone.1), kind=kCustom, calls=%fused_computation.12 | custom fusion | bytes 1576962 | tf_op jit(solution)/shard_map/scatter | solution.py:88
  95.0 1.3 slice.15
  96.3 1.4 all-to-all-done.5
  97.6 8.1 %all-to-all-start.6 = ((bf16[16,24,2048]{2,1,0:T(8,128)(2,1)}), bf16[16,24,2048]{2,1,0:T(8,128)(2,1)S(1)}, u32[]{:S(2)}, u32[]{:S(2)}) async-start(bf16[16,24,2048]{2,1,0:T(8,128)(2,1)} %bitcast.30), calls=%async_computation.6 | async-start | bytes 3145728 | tf_op jit(solution)/shard_map/all_to_all | solution.py:91
  105.7 0.0 all-gather.8.cloned.1.call-start
  105.8 0.7 all-gather.8.cloned.1.call-update
  106.5 0.0 all-gather.4.cloned.1.call-start
  106.5 0.7 all-gather.4.cloned.1.call-update
  107.2 0.0 all-gather.6.cloned.1.call-start
  107.3 0.7 all-gather.6.cloned.1.call-update
  108.0 21.9 %all-gather.8.cloned.1.call-done = bf16[1,1,2,256,1024]{4,3,1,0,2:T(8,128)(2,1)} async-done(((bf16[1,1,1,256,1024]{4,3,1,0,2:T(8,128)(2,1)}), bf16[1,1,2,256,1024]{4,3,1,0,2:T(8,128)(2,1)}) %all-gather.8.cloned.1.call-update) | async-done | bytes 1048592 | tf_op jit(solution)/shard_map/all_gather | solution.py:56
  129.9 2.6 %reshape.125 = bf16[2,4,64,4,256]{4,3,2,1,0:T(4,128)(2,1)} reshape(bf16[1,1,2,256,1024]{4,3,1,0,2:T(8,128)(2,1)} %all-gather.8.cloned.1.call-done) | data formatting | bytes 2097152 | tf_op jit(solution)/shard_map/reshape | solution.py:68
  132.5 2.0 copy.46
  134.6 1.6 squeeze_reshape.3
  136.1 17.2 %all-gather.4.cloned.1.call-done = bf16[1,1,2,128,2048]{4,3,1,0,2:T(8,128)(2,1)} async-done(((bf16[1,1,1,128,2048]{4,3,1,0,2:T(8,128)(2,1)}), bf16[1,1,2,128,2048]{4,3,1,0,2:T(8,128)(2,1)}) %all-gather.4.cloned.1.call-update) | async-done | bytes 1048592 | tf_op jit(solution)/shard_map/all_gather | solution.py:54
  153.3 0.0 all-to-all-done.6
  153.3 1.8 fusion.15
  155.2 21.6 %all-gather.6.cloned.1.call-done = bf16[1,1,2,128,2048]{4,3,1,0,2:T(8,128)(2,1)} async-done(((bf16[1,1,1,128,2048]{4,3,1,0,2:T(8,128)(2,1)}), bf16[1,1,2,128,2048]{4,3,1,0,2:T(8,128)(2,1)}) %all-gather.6.cloned.1.call-update) | async-done | bytes 1048592 | tf_op jit(solution)/shard_map/all_gather | solution.py:55
  176.8 4.5 %convolution_convert_fusion = bf16[384,2048]{1,0:T(8,128)(2,1)} fusion(bf16[256,2048]{1,0:T(8,128)(2,1)} %squeeze_reshape.3, bf16[384,2048]{1,0:T(8,128)(2,1)S(1)} %bitcast.77, bf16[256,2048]{1,0:T(8,128)(2,1)} %bitcast.90, f32[384,256]{1,0:T(8,128)S(1)} %fusion.15), kind=kOutput, calls=%fused_computation.2 | convolution fusion | flops 806682624 | bytes 5636096 | tf_op jit(solution)/shard_map/dot_general | solution.py:96
  181.3 6.6 %all-to-all-start.7 = ((bf16[16,24,2048]{2,1,0:T(8,128)(2,1)}), bf16[16,24,2048]{2,1,0:T(8,128)(2,1)S(1)}, u32[]{:S(2)}, u32[]{:S(2)}) async-start(bf16[16,24,2048]{2,1,0:T(8,128)(2,1)} %bitcast.89), calls=%async_computation.7 | async-start | bytes 3145728 | tf_op jit(solution)/shard_map/all_to_all | solution.py:98
  187.9 0.0 copy-done.5
  187.9 0.1 copy.52
  188.1 2.3 copy.42
  190.3 2.3 copy.38
  192.6 1.6 reshape.126
  194.2 30.0 %all-to-all-done.7 = bf16[16,24,2048]{2,1,0:T(8,128)(2,1)S(1)} async-done(((bf16[16,24,2048]{2,1,0:T(8,128)(2,1)}), bf16[16,24,2048]{2,1,0:T(8,128)(2,1)S(1)}, u32[]{:S(2)}, u32[]{:S(2)}) %all-to-all-start.7) | async-done | bytes 1572896 | tf_op jit(solution)/shard_map/all_to_all | solution.py:98
  224.1 1.2 copy-done
  225.3 1.5 concatenate.3
  226.8 1.4 gather_fusion
  228.2 1.3 reshape.133
  229.5 3.9 %multiply_reduce_fusion = bf16[128,2048]{1,0:T(8,128)(2,1)} fusion(f32[128,2,2048]{2,1,0:T(2,128)S(1)} %reshape.133, f32[128,2]{1,0:T(8,128)S(1)} %copy.52), kind=kLoop, calls=%fused_computation.3 | loop fusion | flops 786432 | bytes 2622464 | tf_op jit(solution)/shard_map/reduce_sum | solution.py:103
  (16 shorter events, 0.1 us)
Async XLA Ops:
  9.8 22.0 %copy-start.4 = (f32[16,64,256]{2,1,0:T(8,128)S(1)}, f32[16,64,256]{2,1,0:T(8,128)}, u32[]{:S(2)}) copy-start(f32[16,64,256]{2,1,0:T(8,128)} %param.12) | copy-start | bytes 3145732
  26.4 22.9 %copy-start.7 = (s32[128]{0:T(128)S(1)}, s32[128]{0:T(128)}, u32[]{:S(2)}) copy-start(s32[128]{0:T(128)} %param.13) | copy-start | bytes 1540
  26.4 22.9 %copy-start.6 = (s32[128,2]{0,1:T(2,128)S(1)}, s32[128,2]{0,1:T(2,128)}, u32[]{:S(2)}) copy-start(s32[128,2]{0,1:T(2,128)} %param.14) | copy-start | bytes 3076
  26.4 15.9 %all-to-all-start.2 = ((bf16[4,4,1,32,512]{4,3,1,2,0:T(8,128)(2,1)}), bf16[4,4,1,32,512]{4,3,1,2,0:T(8,128)(2,1)S(1)}, u32[]{:S(2)}, u32[]{:S(2)}) async-start(bf16[4,4,1,32,512]{4,3,1,2,0:T(8,128)(2,1)} %bitcast.11), calls=%async_computation.2 | async-start | bytes 1048576 | tf_op jit(solution)/shard_map/all_to_all | solution.py:39
  42.4 23.6 %copy-start.1 = (bf16[128,2048]{1,0:T(8,128)(2,1)S(1)}, bf16[128,2048]{1,0:T(8,128)(2,1)}, u32[]{:S(2)}) copy-start(bf16[128,2048]{1,0:T(8,128)(2,1)} %param.8) | copy-start | bytes 1572868
  42.4 17.6 %all-to-all-start.4 = ((bf16[4,4,1,64,256]{4,3,1,2,0:T(8,128)(2,1)}), bf16[4,4,1,64,256]{4,3,1,2,0:T(8,128)(2,1)S(1)}, u32[]{:S(2)}, u32[]{:S(2)}) async-start(bf16[4,4,1,64,256]{4,3,1,2,0:T(8,128)(2,1)} %bitcast.20), calls=%async_computation.4 | async-start | bytes 1048576 | tf_op jit(solution)/shard_map/all_to_all | solution.py:46
  60.0 12.3 %all-to-all-start.1 = ((bf16[1,4,1,32,2048]{4,3,2,0,1:T(8,128)(2,1)}), bf16[1,4,1,32,2048]{4,3,2,0,1:T(8,128)(2,1)S(1)}, u32[]{:S(2)}, u32[]{:S(2)}) async-start(bf16[1,4,1,32,2048]{4,3,2,0,1:T(8,128)(2,1)} %bitcast.4), calls=%async_computation.1 | async-start | bytes 1048576 | tf_op jit(solution)/shard_map/all_to_all | solution.py:31
  72.4 12.3 %copy-start.2 = (bf16[1,4,1,32,2048]{4,3,2,0,1:T(8,128)(2,1)}, bf16[1,4,1,32,2048]{4,3,2,0,1:T(8,128)(2,1)S(1)}, u32[]{:S(2)}) copy-start(bf16[1,4,1,32,2048]{4,3,2,0,1:T(8,128)(2,1)S(1)} %all-to-all-done.1) | copy-start | bytes 1572868
  72.4 12.3 %all-to-all-start.3 = ((bf16[1,4,1,32,2048]{4,3,2,0,1:T(8,128)(2,1)}), bf16[1,4,1,32,2048]{4,3,2,0,1:T(8,128)(2,1)S(1)}, u32[]{:S(2)}, u32[]{:S(2)}) async-start(bf16[1,4,1,32,2048]{4,3,2,0,1:T(8,128)(2,1)} %bitcast.87), calls=%async_computation.3 | async-start | bytes 1048576 | tf_op jit(solution)/shard_map/all_to_all | solution.py:38
  84.6 7.7 %copy-start.3 = (bf16[1,4,1,32,2048]{4,3,2,0,1:T(8,128)(2,1)}, bf16[1,4,1,32,2048]{4,3,2,0,1:T(8,128)(2,1)S(1)}, u32[]{:S(2)}) copy-start(bf16[1,4,1,32,2048]{4,3,2,0,1:T(8,128)(2,1)S(1)} %all-to-all-done.3) | copy-start | bytes 1572868
  84.6 13.0 %all-to-all-start.5 = ((bf16[1,4,1,64,1024]{4,3,2,0,1:T(8,128)(2,1)}), bf16[1,4,1,64,1024]{4,3,2,0,1:T(8,128)(2,1)}, u32[]{:S(2)}, u32[]{:S(2)}) async-start(bf16[1,4,1,64,1024]{4,3,2,0,1:T(8,128)(2,1)} %bitcast.23), calls=%async_computation.5 | async-start | bytes 1048576 | tf_op jit(solution)/shard_map/all_to_all | solution.py:45
  97.6 55.7 %all-to-all-start.6 = ((bf16[16,24,2048]{2,1,0:T(8,128)(2,1)}), bf16[16,24,2048]{2,1,0:T(8,128)(2,1)S(1)}, u32[]{:S(2)}, u32[]{:S(2)}) async-start(bf16[16,24,2048]{2,1,0:T(8,128)(2,1)} %bitcast.30), calls=%async_computation.6 | async-start | bytes 3145728 | tf_op jit(solution)/shard_map/all_to_all | solution.py:91
  105.7 24.1 %all-gather.8.cloned.1.call-start = ((), (), s32[]{:S(2)}) async-start(), calls=%async_computation.10 | async-start | bytes 1572864 | tf_op jit(solution)/shard_map/all_gather | solution.py:56
  106.5 46.8 %all-gather.4.cloned.1.call-start = ((), (), s32[]{:S(2)}) async-start(), calls=%async_computation.8 | async-start | bytes 1572864 | tf_op jit(solution)/shard_map/all_gather | solution.py:54
  107.2 69.5 %all-gather.6.cloned.1.call-start = ((), (), s32[]{:S(2)}) async-start(), calls=%async_computation.9 | async-start | bytes 1572864 | tf_op jit(solution)/shard_map/all_gather | solution.py:55
  181.3 6.6 %copy-start.5 = (f32[128,2]{0,1:T(2,128)S(1)}, f32[128,2]{0,1:T(2,128)}, u32[]{:S(2)}) copy-start(f32[128,2]{0,1:T(2,128)} %param.15) | copy-start | bytes 3076
  181.3 42.8 %all-to-all-start.7 = ((bf16[16,24,2048]{2,1,0:T(8,128)(2,1)}), bf16[16,24,2048]{2,1,0:T(8,128)(2,1)S(1)}, u32[]{:S(2)}, u32[]{:S(2)}) async-start(bf16[16,24,2048]{2,1,0:T(8,128)(2,1)} %bitcast.89), calls=%async_computation.7 | async-start | bytes 3145728 | tf_op jit(solution)/shard_map/all_to_all | solution.py:98
  224.1 1.2 copy-start
Sparse Core Ops, SparseCore 0:
  108.1 21.7 all-gather.7
  132.0 21.2 all-gather.3
  155.4 21.2 all-gather.5
where the time goes:
time: 241 us; the launch traced here: 240 us
  waiting for transfers between devices  125 us (52%)
  starting transfers between devices  43.7 us (18%)
  local copies, waits for them, and re-layouts  26.2 us (11%)
  blocking collectives  16.6 us (7%)
  between operations  13.9 us (6%)
  other arithmetic  8.49 us (4%)
  matrix products  6.36 us (3%)
    all_to_all x1, waiting for transfers between devices, body(): lax.all_to_all(outcome, ('fs', 'tp'), split_axis=0, concat_axis=0, tiled=...  30 us
    all_gather x1, waiting for transfers between devices, body(): lax.all_gather(grids[2], 'gr', axis=2, tiled=True)  21.9 us
    all_gather x1, waiting for transfers between devices, body(): lax.all_gather(grids[1], 'gr', axis=2, tiled=True)  21.6 us
    all_gather x1, waiting for transfers between devices, body(): lax.all_gather(grids[0], 'gr', axis=2, tiled=True)  17.2 us
    all_to_all x1, blocking collectives, body(): lax.all_to_all(grids[0], 'fs', split_axis=0, concat_axis=4, tiled=True)  16.6 us
    all_to_all x1, waiting for transfers between devices, body(): lax.all_to_all(grids[1], 'fs', split_axis=0, concat_axis=4, tiled=True)  9.78 us
    all_to_all x1, waiting for transfers between devices, body(): lax.all_to_all(grids[2], 'fs', split_axis=0, concat_axis=4, tiled=True)  9.51 us
    all_to_all x1, starting transfers between devices, body(): lax.all_to_all(outgoing, ('fs', 'tp'), split_axis=0, concat_axis=0, tiled...  8.1 us
  transfers between devices with their start and end apart: 10, of which 9 were waited for; matrix products, arithmetic and copies ran while one was open for 10% of the time, Pallas kernels for 0%

commit v1 on v0

--- a/solution.py
+++ b/solution.py
@@ -52,7 +52,9 @@
     )
     grids = (
         lax.all_gather(grids[0], "gr", axis=2, tiled=True),
-        lax.all_gather(grids[1], "gr", axis=2, tiled=True),
+        jnp.concatenate(
+            lax.all_to_all(jnp.stack(lax.axis_size("gr") * [grids[1]], axis=0), "gr", 0, 0), axis=2
+        ),
         lax.all_gather(grids[2], "gr", axis=2, tiled=True),
     )
 

time: 241 us -> 229 us (0.950)
  waiting for transfers between devices: 125 us -> 107 us
  starting transfers between devices: 43.7 us -> 47.8 us
    all_to_all x1, waiting for transfers between devices: 0.01 us -> 33.7 us  [body(): lax.all_to_all(outgoing, ('fs', 'tp'), split_axis=0, concat_axis=0, tiled...]
    all_gather x1, waiting for transfers between devices: 21.9 us -> 0.02 us  [body(): lax.all_gather(grids[2], 'gr', axis=2, tiled=True)]
    all_gather x1 -> x0, waiting for transfers between devices: 21.6 us -> none  [body(): lax.all_gather(grids[1], 'gr', axis=2, tiled=True)]
    all_gather x1, waiting for transfers between devices: 17.2 us -> 4.16 us  [body(): lax.all_gather(grids[0], 'gr', axis=2, tiled=True)]
    all_to_all x0 -> x1, waiting for transfers between devices: none -> 6.1 us  [body(): lax.all_to_all(jnp.stack(lax.axis_size('gr') * [grids[1]], axis=0), 'gr',...]
    all_to_all x0 -> x1, starting transfers between devices: none -> 4.42 us  [body(): lax.all_to_all(jnp.stack(lax.axis_size('gr') * [grids[1]], axis=0), 'gr',...]
  transfers between devices with their start and end apart: 10 -> 10, of which waited for: 9 -> 9; matrix products, arithmetic and copies ran while one was open for 10% -> 11% of each run, Pallas kernels for 0% -> 0%
where the time goes in v1:
time: 229 us; the launch traced here: 228 us
  waiting for transfers between devices  107 us (47%)
  starting transfers between devices  47.8 us (21%)
  local copies, waits for them, and re-layouts  26.2 us (11%)
  blocking collectives  16.6 us (7%)
  between operations  14.2 us (6%)
  other arithmetic  9.55 us (4%)
  matrix products  6.38 us (3%)
    all_to_all x1, waiting for transfers between devices, body(): lax.all_to_all(outgoing, ('fs', 'tp'), split_axis=0, concat_axis=0, tiled...  33.7 us
    all_to_all x1, waiting for transfers between devices, body(): lax.all_to_all(outcome, ('fs', 'tp'), split_axis=0, concat_axis=0, tiled=...  30 us
    all_to_all x1, blocking collectives, body(): lax.all_to_all(grids[0], 'fs', split_axis=0, concat_axis=4, tiled=True)  16.6 us
    all_to_all x1, waiting for transfers between devices, body(): lax.all_to_all(grids[1], 'fs', split_axis=0, concat_axis=4, tiled=True)  9.78 us
    all_to_all x1, waiting for transfers between devices, body(): lax.all_to_all(grids[2], 'fs', split_axis=0, concat_axis=4, tiled=True)  9.51 us
    all_to_all x1, starting transfers between devices, body(): lax.all_to_all(outgoing, ('fs', 'tp'), split_axis=0, concat_axis=0, tiled...  8.1 us
    all_to_all x1, starting transfers between devices, body(): lax.all_to_all(grids[2], 'fs', split_axis=0, concat_axis=4, tiled=True)  6.98 us
    all_to_all x1, starting transfers between devices, body(): lax.all_to_all(outcome, ('fs', 'tp'), split_axis=0, concat_axis=0, tiled=...  6.28 us
  transfers between devices with their start and end apart: 10, of which 9 were waited for; matrix products, arithmetic and copies ran while one was open for 11% of the time, Pallas kernels for 0%

profile of v1, /device:TPU:13, one launch (start us, length us, event | category | flops | bytes accessed | tf_op | source)
XLA Modules:
  0.0 227.9 jit_solution(7191702039318484158)
XLA Ops:
  7.2 2.6 %multiply_convert_fusion = (bf16[16,512,32]{1,2,0:T(8,128)(2,1)}, bf16[16,512,32]{1,2,0:T(8,128)(2,1)S(1)}) fusion(f32[16,512,32]{1,2,0:T(8,128)} %param.11, f32[512]{0:T(512)} %param.9, f32[16,512,32]{1,2,0:T(8,128)} %param.10), kind=kLoop, calls=%fused_computation.11 | loop fusion | flops 1048576 | bytes 3147776 | tf_op jit(solution)/shard_map/convert_element_type | solution.py:19
  9.8 0.0 copy-start.3
  9.8 16.6 %all_to_all.102 = bf16[4,4,1,32,512]{4,3,1,2,0:T(8,128)(2,1)S(1)} all-to-all(bf16[4,4,1,32,512]{4,3,1,2,0:T(8,128)(2,1)S(1)} %bitcast.86), channel_id=1, replica_groups=mesh['gr'=2,'fs'=4,'tp'=4] {'fs'}, dimensions={0} | all-to-all | bytes 1048576 | tf_op jit(solution)/shard_map/all_to_all | solution.py:32
  26.4 5.3 %all-to-all-start.2 = ((bf16[4,4,1,32,512]{4,3,1,2,0:T(8,128)(2,1)}), bf16[4,4,1,32,512]{4,3,1,2,0:T(8,128)(2,1)S(1)}, u32[]{:S(2)}, u32[]{:S(2)}) async-start(bf16[4,4,1,32,512]{4,3,1,2,0:T(8,128)(2,1)} %bitcast.11), calls=%async_computation.2 | async-start | bytes 1048576 | tf_op jit(solution)/shard_map/all_to_all | solution.py:39
  31.7 0.0 copy-done.3
  31.7 0.9 convert_element_type.37
  32.6 9.8 %all-to-all-done.2 = bf16[4,4,1,32,512]{4,3,1,2,0:T(8,128)(2,1)S(1)} async-done(((bf16[4,4,1,32,512]{4,3,1,2,0:T(8,128)(2,1)}), bf16[4,4,1,32,512]{4,3,1,2,0:T(8,128)(2,1)S(1)}, u32[]{:S(2)}, u32[]{:S(2)}) %all-to-all-start.2) | async-done | bytes 524320 | tf_op jit(solution)/shard_map/all_to_all | solution.py:39
  42.4 7.0 %all-to-all-start.5 = ((bf16[4,4,1,64,256]{4,3,1,2,0:T(8,128)(2,1)}), bf16[4,4,1,64,256]{4,3,1,2,0:T(8,128)(2,1)S(1)}, u32[]{:S(2)}, u32[]{:S(2)}) async-start(bf16[4,4,1,64,256]{4,3,1,2,0:T(8,128)(2,1)} %bitcast.19), calls=%async_computation.5 | async-start | bytes 1048576 | tf_op jit(solution)/shard_map/all_to_all | solution.py:46
  49.4 0.0 copy-done.6
  49.4 0.0 copy-done.5
  49.4 0.1 copy.46
  49.5 0.1 eq.21
  49.6 0.9 copy.52
  50.5 9.5 %all-to-all-done.5 = bf16[4,4,1,64,256]{4,3,1,2,0:T(8,128)(2,1)S(1)} async-done(((bf16[4,4,1,64,256]{4,3,1,2,0:T(8,128)(2,1)}), bf16[4,4,1,64,256]{4,3,1,2,0:T(8,128)(2,1)S(1)}, u32[]{:S(2)}, u32[]{:S(2)}) %all-to-all-start.5) | async-done | bytes 524320 | tf_op jit(solution)/shard_map/all_to_all | solution.py:46
  60.0 5.4 %all-to-all-start.1 = ((bf16[1,4,1,32,2048]{4,3,2,0,1:T(8,128)(2,1)}), bf16[1,4,1,32,2048]{4,3,2,0,1:T(8,128)(2,1)S(1)}, u32[]{:S(2)}, u32[]{:S(2)}) async-start(bf16[1,4,1,32,2048]{4,3,2,0,1:T(8,128)(2,1)} %bitcast.4), calls=%async_computation.1 | async-start | bytes 1048576 | tf_op jit(solution)/shard_map/all_to_all | solution.py:31
  65.4 0.6 reduce-window.6
  66.0 0.0 copy-done.1
  66.0 0.2 fusion.1
  66.2 0.9 copy.53
  67.0 5.3 %all-to-all-done.1 = bf16[1,4,1,32,2048]{4,3,2,0,1:T(8,128)(2,1)S(1)} async-done(((bf16[1,4,1,32,2048]{4,3,2,0,1:T(8,128)(2,1)}), bf16[1,4,1,32,2048]{4,3,2,0,1:T(8,128)(2,1)S(1)}, u32[]{:S(2)}, u32[]{:S(2)}) %all-to-all-start.1) | async-done | bytes 524320 | tf_op jit(solution)/shard_map/all_to_all | solution.py:31
  72.4 5.3 %all-to-all-start.3 = ((bf16[1,4,1,32,2048]{4,3,2,0,1:T(8,128)(2,1)}), bf16[1,4,1,32,2048]{4,3,2,0,1:T(8,128)(2,1)S(1)}, u32[]{:S(2)}, u32[]{:S(2)}) async-start(bf16[1,4,1,32,2048]{4,3,2,0,1:T(8,128)(2,1)} %bitcast.85), calls=%async_computation.3 | async-start | bytes 1048576 | tf_op jit(solution)/shard_map/all_to_all | solution.py:38
  77.6 0.2 fusion.2
  77.8 0.9 copy.54
  78.7 6.0 %all-to-all-done.3 = bf16[1,4,1,32,2048]{4,3,2,0,1:T(8,128)(2,1)S(1)} async-done(((bf16[1,4,1,32,2048]{4,3,2,0,1:T(8,128)(2,1)}), bf16[1,4,1,32,2048]{4,3,2,0,1:T(8,128)(2,1)S(1)}, u32[]{:S(2)}, u32[]{:S(2)}) %all-to-all-start.3) | async-done | bytes 524320 | tf_op jit(solution)/shard_map/all_to_all | solution.py:38
  84.6 0.0 copy-done.2
  84.6 5.9 %all-to-all-start.6 = ((bf16[1,4,1,64,1024]{4,3,2,0,1:T(8,128)(2,1)}), bf16[1,4,1,64,1024]{4,3,2,0,1:T(8,128)(2,1)}, u32[]{:S(2)}, u32[]{:S(2)}) async-start(bf16[1,4,1,64,1024]{4,3,2,0,1:T(8,128)(2,1)} %bitcast.22), calls=%async_computation.6 | async-start | bytes 1048576 | tf_op jit(solution)/shard_map/all_to_all | solution.py:45
  90.6 0.2 slice_reduce_fusion
  90.7 0.1 eq.18
  90.9 0.1 copy.49
  91.0 0.1 mul.70
  91.2 0.6 broadcast_in_dim.28
  91.8 0.4 reshape.143
  92.3 0.1 fusion.12
  92.4 2.6 %scatter_custom_fusion = bf16[385,2048]{1,0:T(8,128)(2,1)S(1)} fusion(s32[256]{0:T(256)S(1)} %bitcast.90, bf16[256,2048]{1,0:T(8,128)(2,1)S(1)} %reshape.143, bf16[]{:T(256)} %constant.11.clone.1), kind=kCustom, calls=%fused_computation.13 | custom fusion | bytes 1576962 | tf_op jit(solution)/shard_map/scatter | solution.py:90
  95.0 1.3 slice.15
  96.3 1.4 all-to-all-done.6
  97.6 8.1 %all-to-all-start.7 = ((bf16[16,24,2048]{2,1,0:T(8,128)(2,1)}), bf16[16,24,2048]{2,1,0:T(8,128)(2,1)S(1)}, u32[]{:S(2)}, u32[]{:S(2)}) async-start(bf16[16,24,2048]{2,1,0:T(8,128)(2,1)} %bitcast.29), calls=%async_computation.7 | async-start | bytes 3145728 | tf_op jit(solution)/shard_map/all_to_all | solution.py:93
  105.7 0.0 all-gather.5.cloned.1.call-start
  105.8 0.7 all-gather.5.cloned.1.call-update
  106.5 0.0 all-gather.3.cloned.1.call-start
  106.5 0.7 all-gather.3.cloned.1.call-update
  107.2 1.1 pad_maximum_fusion
  108.3 33.7 %all-to-all-done.7 = bf16[16,24,2048]{2,1,0:T(8,128)(2,1)S(1)} async-done(((bf16[16,24,2048]{2,1,0:T(8,128)(2,1)}), bf16[16,24,2048]{2,1,0:T(8,128)(2,1)S(1)}, u32[]{:S(2)}, u32[]{:S(2)}) %all-to-all-start.7) | async-done | bytes 1572896 | tf_op jit(solution)/shard_map/all_to_all | solution.py:93
  141.9 4.4 %all-to-all-start.4 = ((bf16[2,1,1,1,128,2048]{5,4,3,2,1,0:T(8,128)(2,1)}), bf16[2,1,1,1,128,2048]{5,4,3,2,1,0:T(8,128)(2,1)}, u32[]{:S(2)}, u32[]{:S(2)}) async-start(bf16[2,1,1,1,128,2048]{5,4,3,2,1,0:T(8,128)(2,1)} %pad_maximum_fusion), calls=%async_computation.4 | async-start | bytes 2097152 | tf_op jit(solution)/shard_map/all_to_all | solution.py:56
  146.4 0.0 all-gather.5.cloned.1.call-done
  146.4 2.6 %reshape.122 = bf16[2,4,64,4,256]{4,3,2,1,0:T(4,128)(2,1)} reshape(bf16[1,1,2,256,1024]{4,3,1,0,2:T(8,128)(2,1)} %all-gather.5.cloned.1.call-done) | data formatting | bytes 2097152 | tf_op jit(solution)/shard_map/reshape | solution.py:70
  149.0 2.0 copy.45
  151.1 1.6 squeeze_reshape.3
  152.6 4.2 %all-gather.3.cloned.1.call-done = bf16[1,1,2,128,2048]{4,3,1,0,2:T(8,128)(2,1)} async-done(((bf16[1,1,1,128,2048]{4,3,1,0,2:T(8,128)(2,1)}), bf16[1,1,2,128,2048]{4,3,1,0,2:T(8,128)(2,1)}) %all-gather.3.cloned.1.call-update) | async-done | bytes 1048592 | tf_op jit(solution)/shard_map/all_gather | solution.py:54
  156.8 1.8 fusion.15
  158.6 6.1 %all-to-all-done.4 = bf16[2,1,1,1,128,2048]{5,4,3,2,1,0:T(8,128)(2,1)} async-done(((bf16[2,1,1,1,128,2048]{5,4,3,2,1,0:T(8,128)(2,1)}), bf16[2,1,1,1,128,2048]{5,4,3,2,1,0:T(8,128)(2,1)}, u32[]{:S(2)}, u32[]{:S(2)}) %all-to-all-start.4) | async-done | bytes 1048608 | tf_op jit(solution)/shard_map/all_to_all | solution.py:56
  164.7 4.5 %convolution_convert_fusion = bf16[384,2048]{1,0:T(8,128)(2,1)} fusion(bf16[256,2048]{1,0:T(8,128)(2,1)} %squeeze_reshape.3, bf16[384,2048]{1,0:T(8,128)(2,1)S(1)} %bitcast.75, bf16[256,2048]{1,0:T(8,128)(2,1)} %bitcast.16, f32[384,256]{1,0:T(8,128)S(1)} %fusion.15), kind=kOutput, calls=%fused_computation.2 | convolution fusion | flops 806682624 | bytes 5636096 | tf_op jit(solution)/shard_map/dot_general | solution.py:98
  169.3 6.3 %all-to-all-start.8 = ((bf16[16,24,2048]{2,1,0:T(8,128)(2,1)}), bf16[16,24,2048]{2,1,0:T(8,128)(2,1)S(1)}, u32[]{:S(2)}, u32[]{:S(2)}) async-start(bf16[16,24,2048]{2,1,0:T(8,128)(2,1)} %bitcast.87), calls=%async_computation.8 | async-start | bytes 3145728 | tf_op jit(solution)/shard_map/all_to_all | solution.py:100
  175.6 0.0 copy-done.4
  175.6 0.1 copy.51
  175.7 2.3 copy.41
  178.0 2.3 copy.38
  180.2 1.6 reshape.123
  181.8 30.0 %all-to-all-done.8 = bf16[16,24,2048]{2,1,0:T(8,128)(2,1)S(1)} async-done(((bf16[16,24,2048]{2,1,0:T(8,128)(2,1)}), bf16[16,24,2048]{2,1,0:T(8,128)(2,1)S(1)}, u32[]{:S(2)}, u32[]{:S(2)}) %all-to-all-start.8) | async-done | bytes 1572896 | tf_op jit(solution)/shard_map/all_to_all | solution.py:100
  211.8 1.2 copy-done
  212.9 1.5 concatenate.3
  214.4 1.4 gather_fusion
  215.8 1.3 reshape.130
  217.2 3.9 %multiply_reduce_fusion = bf16[128,2048]{1,0:T(8,128)(2,1)} fusion(f32[128,2,2048]{2,1,0:T(2,128)S(1)} %reshape.130, f32[128,2]{1,0:T(8,128)S(1)} %copy.51), kind=kLoop, calls=%fused_computation.3 | loop fusion | flops 786432 | bytes 2622464 | tf_op jit(solution)/shard_map/reduce_sum | solution.py:105
  (14 shorter events, 0.1 us)
Async XLA Ops:
  9.8 22.0 %copy-start.3 = (f32[16,64,256]{2,1,0:T(8,128)S(1)}, f32[16,64,256]{2,1,0:T(8,128)}, u32[]{:S(2)}) copy-start(f32[16,64,256]{2,1,0:T(8,128)} %param.12) | copy-start | bytes 3145732
  26.4 22.9 %copy-start.6 = (s32[128]{0:T(128)S(1)}, s32[128]{0:T(128)}, u32[]{:S(2)}) copy-start(s32[128]{0:T(128)} %param.13) | copy-start | bytes 1540
  26.4 22.9 %copy-start.5 = (s32[128,2]{0,1:T(2,128)S(1)}, s32[128,2]{0,1:T(2,128)}, u32[]{:S(2)}) copy-start(s32[128,2]{0,1:T(2,128)} %param.14) | copy-start | bytes 3076
  26.4 15.9 %all-to-all-start.2 = ((bf16[4,4,1,32,512]{4,3,1,2,0:T(8,128)(2,1)}), bf16[4,4,1,32,512]{4,3,1,2,0:T(8,128)(2,1)S(1)}, u32[]{:S(2)}, u32[]{:S(2)}) async-start(bf16[4,4,1,32,512]{4,3,1,2,0:T(8,128)(2,1)} %bitcast.11), calls=%async_computation.2 | async-start | bytes 1048576 | tf_op jit(solution)/shard_map/all_to_all | solution.py:39
  42.4 23.6 %copy-start.1 = (bf16[128,2048]{1,0:T(8,128)(2,1)S(1)}, bf16[128,2048]{1,0:T(8,128)(2,1)}, u32[]{:S(2)}) copy-start(bf16[128,2048]{1,0:T(8,128)(2,1)} %param.8) | copy-start | bytes 1572868
  42.4 17.6 %all-to-all-start.5 = ((bf16[4,4,1,64,256]{4,3,1,2,0:T(8,128)(2,1)}), bf16[4,4,1,64,256]{4,3,1,2,0:T(8,128)(2,1)S(1)}, u32[]{:S(2)}, u32[]{:S(2)}) async-start(bf16[4,4,1,64,256]{4,3,1,2,0:T(8,128)(2,1)} %bitcast.19), calls=%async_computation.5 | async-start | bytes 1048576 | tf_op jit(solution)/shard_map/all_to_all | solution.py:46
  60.0 12.3 %all-to-all-start.1 = ((bf16[1,4,1,32,2048]{4,3,2,0,1:T(8,128)(2,1)}), bf16[1,4,1,32,2048]{4,3,2,0,1:T(8,128)(2,1)S(1)}, u32[]{:S(2)}, u32[]{:S(2)}) async-start(bf16[1,4,1,32,2048]{4,3,2,0,1:T(8,128)(2,1)} %bitcast.4), calls=%async_computation.1 | async-start | bytes 1048576 | tf_op jit(solution)/shard_map/all_to_all | solution.py:31
  72.4 12.3 %copy-start.2 = (bf16[1,4,1,32,2048]{4,3,2,0,1:T(8,128)(2,1)}, bf16[1,4,1,32,2048]{4,3,2,0,1:T(8,128)(2,1)S(1)}, u32[]{:S(2)}) copy-start(bf16[1,4,1,32,2048]{4,3,2,0,1:T(8,128)(2,1)S(1)} %all-to-all-done.1) | copy-start | bytes 1572868
  72.4 12.3 %all-to-all-start.3 = ((bf16[1,4,1,32,2048]{4,3,2,0,1:T(8,128)(2,1)}), bf16[1,4,1,32,2048]{4,3,2,0,1:T(8,128)(2,1)S(1)}, u32[]{:S(2)}, u32[]{:S(2)}) async-start(bf16[1,4,1,32,2048]{4,3,2,0,1:T(8,128)(2,1)} %bitcast.85), calls=%async_computation.3 | async-start | bytes 1048576 | tf_op jit(solution)/shard_map/all_to_all | solution.py:38
  84.6 13.0 %all-to-all-start.6 = ((bf16[1,4,1,64,1024]{4,3,2,0,1:T(8,128)(2,1)}), bf16[1,4,1,64,1024]{4,3,2,0,1:T(8,128)(2,1)}, u32[]{:S(2)}, u32[]{:S(2)}) async-start(bf16[1,4,1,64,1024]{4,3,2,0,1:T(8,128)(2,1)} %bitcast.22), calls=%async_computation.6 | async-start | bytes 1048576 | tf_op jit(solution)/shard_map/all_to_all | solution.py:45
  97.6 44.3 %all-to-all-start.7 = ((bf16[16,24,2048]{2,1,0:T(8,128)(2,1)}), bf16[16,24,2048]{2,1,0:T(8,128)(2,1)S(1)}, u32[]{:S(2)}, u32[]{:S(2)}) async-start(bf16[16,24,2048]{2,1,0:T(8,128)(2,1)} %bitcast.29), calls=%async_computation.7 | async-start | bytes 3145728 | tf_op jit(solution)/shard_map/all_to_all | solution.py:93
  105.7 40.7 %all-gather.5.cloned.1.call-start = ((), (), s32[]{:S(2)}) async-start(), calls=%async_computation.10 | async-start | bytes 1572864 | tf_op jit(solution)/shard_map/all_gather | solution.py:58
  106.5 50.4 %all-gather.3.cloned.1.call-start = ((), (), s32[]{:S(2)}) async-start(), calls=%async_computation.9 | async-start | bytes 1572864 | tf_op jit(solution)/shard_map/all_gather | solution.py:54
  141.9 22.8 %all-to-all-start.4 = ((bf16[2,1,1,1,128,2048]{5,4,3,2,1,0:T(8,128)(2,1)}), bf16[2,1,1,1,128,2048]{5,4,3,2,1,0:T(8,128)(2,1)}, u32[]{:S(2)}, u32[]{:S(2)}) async-start(bf16[2,1,1,1,128,2048]{5,4,3,2,1,0:T(8,128)(2,1)} %pad_maximum_fusion), calls=%async_computation.4 | async-start | bytes 2097152 | tf_op jit(solution)/shard_map/all_to_all | solution.py:56
  169.3 6.3 %copy-start.4 = (f32[128,2]{0,1:T(2,128)S(1)}, f32[128,2]{0,1:T(2,128)}, u32[]{:S(2)}) copy-start(f32[128,2]{0,1:T(2,128)} %param.15) | copy-start | bytes 3076
  169.3 42.5 %all-to-all-start.8 = ((bf16[16,24,2048]{2,1,0:T(8,128)(2,1)}), bf16[16,24,2048]{2,1,0:T(8,128)(2,1)S(1)}, u32[]{:S(2)}, u32[]{:S(2)}) async-start(bf16[16,24,2048]{2,1,0:T(8,128)(2,1)} %bitcast.87), calls=%async_computation.8 | async-start | bytes 3145728 | tf_op jit(solution)/shard_map/all_to_all | solution.py:100
  211.8 1.2 copy-start
Sparse Core Ops, SparseCore 0:
  108.1 21.7 all-gather.4
  132.0 24.7 all-gather.2
